TPU v7x, 32 devices: a whole 2x2x4 slice. The times are simulated.
32 devices in a mesh: ep: 16 (over z, y, x), tp: 2 (over core).
Axes of the slice: x: 2, y: 2, z: 4, core: 2. Of those that a mesh axis runs over, the one named last changes fastest.
Arguments:
- tokens: bfloat16 [4096, 4096], P('ep'), may hold values from -6 to 6
- cotangent: bfloat16 [4096, 4096], P('ep'), may hold values from -1.5 to 1.5
- gates: float32 [4096, 2], P('ep'), may hold values from 0.05 to 0.95
- experts: int32 [4096, 2], P('ep'), may hold values from 0 to 15, all different within a row; in each aligned block of 256 rows (0 to 255, 256 to 511, ...) at most 48 rows name the same one
- gate_w: bfloat16 [16, 4096, 768], P('ep', None, 'tp'), may hold values from -0.09375 to 0.09375
- up_w: bfloat16 [16, 4096, 768], P('ep', None, 'tp'), may hold values from -0.09375 to 0.09375
- down_w: bfloat16 [16, 768, 4096], P('ep', 'tp'), may hold values from -0.21875 to 0.21875
Outputs:
- grad_tokens: bfloat16 [4096, 4096], P('ep', 'tp')
- grad_gates: float32 [4096, 2], P('ep')
- grad_gate_w: bfloat16 [16, 4096, 768], P('ep', None, 'tp')
- grad_up_w: bfloat16 [16, 4096, 768], P('ep', None, 'tp')
- grad_down_w: bfloat16 [16, 768, 4096], P('ep', 'tp')
- sq_gate: float32 [16, 4096], P('ep')
- sq_up: float32 [16, 4096], P('ep')
- sq_down: float32 [16, 768], P('ep', 'tp')
Inputs may be any that keep to these rules, and one draw needn't show every extreme that they name: In each aligned block of 256 rows no expert is named by more than 48 rows, a bound that some expert reaches in some blocks; the 2 experts of a row differ.
All inputs are finite; a program needn't handle non-finite values.
Results may differ from a plain program's by a relative error of at most 0.024.
Values may be sent and summed in bfloat16 or wider, within the bound.
A program may use at most 192 MiB of HBM per device.

v0:
```python
import functools

import jax
import jax.numpy as jnp
from jax import lax
from jax.experimental import pallas as pl
from jax.experimental.pallas import tpu as pltpu
from jax.sharding import PartitionSpec as P

MESH = pl.DeviceIdType.MESH
BF16 = jnp.bfloat16
F32 = jnp.float32
NN = (((1,), (0,)), ((), ()))
NT = (((1,), (1,)), ((), ()))
TN = (((0,), (0,)), ((), ()))


def dot(a, b, dims, precision=None):
    return lax.dot_general(a, b, dims, precision=precision, preferred_element_type=F32)


def kernel(
    n, cap, units, share, groups, tile,
    sx, sdy, sg, wg_in, wu_in, wd_in,
    back, gback, ggw, guw, gdw, sq_out, sqd_out,
    xr, dyr, gr, wg, wu, wd, pg, pu, prod, gpgu, wt, keep, give, got, rg,
    gp, gpp, gt, gcol, sqs, sqr, acc,
    w_sem, s_sem, r_sem, gs_sem, gr_sem, fs_sem, fr_sem,
    ps_sem, pr_sem, qs_sem, qr_sem, bs_sem, br_sem, hs_sem, hr_sem, o_sem, e_sem,
):
    me = lax.axis_index("ep")
    t = lax.axis_index("tp")
    other = lax.axis_size("tp") - 1 - t
    per = n // groups
    rows_g = per * cap

    def rows(s):
        return pl.ds(pl.multiple_of(s * cap, 16), cap)

    def remote(src, dst, send, recv, **where):
        return pltpu.make_async_remote_copy(
            src_ref=src, dst_ref=dst, send_sem=send, recv_sem=recv,
            device_id=where, device_id_type=MESH,
        )

    def loop(count, fn):
        def step(i, carry):
            fn(i)
            return carry
        lax.fori_loop(0, count, step, 0)

    def peer(k):
        return lax.rem(me + n // 2 + k + jnp.where(k >= n - n // 2, 1, 0), n)

    barrier = pltpu.get_barrier_semaphore()
    loop(n - 1, lambda k: pl.semaphore_signal(
        barrier, inc=1, device_id={"ep": peer(k)}, device_id_type=MESH))
    pl.semaphore_signal(barrier, inc=1, device_id={"tp": other}, device_id_type=MESH)
    pl.semaphore_wait(barrier, n)

    ins = ((sx, xr), (sdy, dyr))
    for which, (src, dst) in enumerate(ins):
        def send(k, which=which, src=src, dst=dst):
            d = peer(k)
            remote(src.at[d], dst.at[t, rows(me)], s_sem.at[which, d],
                   r_sem.at[which, me], ep=d).start()
        loop(n - 1, send)
        pltpu.make_async_copy(src.at[me], dst.at[t, rows(me)], r_sem.at[which, me]).start()
        if which == 0:
            def send_gate(k):
                d = peer(k)
                remote(sg.at[d], gr.at[me], gs_sem.at[d], gr_sem.at[me], ep=d).start()
            loop(n - 1, send_gate)
            pltpu.make_async_copy(sg.at[me], gr.at[me], gr_sem.at[me]).start()
            loads = [
                pltpu.make_async_copy(a, b, w_sem.at[i])
                for i, (a, b) in enumerate(((wg_in, wg), (wu_in, wu), (wd_in, wd)))
            ]
            for load in loads:
                load.start()

    def order(i):
        return lax.rem(me // per + groups // 2 + i, groups)

    def arrive(which, g):
        src, dst = ins[which]

        def pass_on(j):
            s = g * per + j
            pltpu.make_async_copy(src.at[0], dst.at[t, rows(s)], r_sem.at[which, s]).wait()
            remote(dst.at[t, rows(s)], dst.at[t, rows(s)], fs_sem.at[which, s],
                   fr_sem.at[which, s], tp=other).start()

        def joined(j):
            s = g * per + j
            remote(dst.at[other, rows(s)], dst.at[other, rows(s)], fs_sem.at[which, s],
                   fr_sem.at[which, s], tp=other).wait_recv()

        loop(per, pass_on)
        loop(per, joined)

    def span(g):
        return pl.ds(pl.multiple_of(g * rows_g, 16), rows_g)

    for load in loads:
        load.wait()

    def forward(i):
        g = order(i)
        arrive(0, g)
        r = span(g)
        pg[r, :] = dot(xr[0, r, :], wg[0], NN) + dot(xr[1, r, :], wg[1], NN)
        pu[r, :] = dot(xr[0, r, :], wu[0], NN) + dot(xr[1, r, :], wu[1], NN)

    loop(groups, forward)

    def exchange(g):
        r = span(g)
        grp = pl.ds(g * per, per)
        return (
            remote(give.at[r], got.at[r], ps_sem.at[g], pr_sem.at[g], tp=other),
            remote(gp.at[grp], gpp.at[grp], qs_sem.at[g], qr_sem.at[g], tp=other),
        )

    def back_copies(s):
        return (
            remote(rg.at[rows(s)], back.at[me], bs_sem.at[s], br_sem.at[me], ep=s),
            remote(gt.at[s], gback.at[me], hs_sem.at[s], hr_sem.at[me], ep=s),
        )

    def finish(g):
        for copy in exchange(g):
            copy.wait_recv()

        def one(j):
            s = g * per + j
            r = rows(s)
            rg[r, :] = (keep[r, :].astype(F32) + got[r, :].astype(F32)).astype(BF16)
            gt[s] = gp[s] + gpp[s]

        loop(per, one)

        def out(j):
            s = g * per + j

            @pl.when(s == me)
            def _():
                pltpu.make_async_copy(rg.at[rows(s)], back.at[me], br_sem.at[me]).start()
                pltpu.make_async_copy(gt.at[s], gback.at[me], hr_sem.at[me]).start()

            @pl.when(s != me)
            def _():
                for copy in back_copies(s):
                    copy.start()

        loop(per, out)

    ones_units = jnp.ones((8, units), F32)

    def backward(i):
        g = order(i)
        arrive(1, g)

        def gates_in(j):
            s = g * per + j
            pltpu.make_async_copy(sg.at[0], gr.at[s], gr_sem.at[s]).wait()
            column = jnp.transpose(gr[s])
            gcol[rows(s), :] = jnp.broadcast_to(column[:cap, 0:1], (cap, 128))

        loop(per, gates_in)
        r = span(g)
        dh = dot(dyr[0, r, :], wd[:, :share], NT) + dot(dyr[1, r, :], wd[:, share:], NT)
        a = pg[r, :]
        b = pu[r, :]
        gate = gcol[r, 0:1]
        sig = jax.nn.sigmoid(a)
        silu = a * sig
        hidden = (silu * b).astype(BF16).astype(F32)
        prod[...] = hidden * dh
        scaled = gate * dh
        gpg = (scaled * b * sig * (1.0 + a * (1.0 - sig))).astype(BF16)
        gpu = (scaled * silu).astype(BF16)
        gpgu[r, :units] = gpg
        gpgu[r, units:] = gpu
        wt[r, :] = (gate * hidden).astype(BF16)

        def part(c):
            cols = pl.ds(pl.multiple_of(c * tile, tile), tile)
            for half, dst in ((other, give), (t, keep)):
                dst[r, cols] = (
                    dot(gpgu[r, :units], wg[half, cols, :], NT)
                    + dot(gpgu[r, units:], wu[half, cols, :], NT)
                ).astype(BF16)

        loop(share // tile, part)

        def gate_sum(j):
            p = prod[pl.ds(pl.multiple_of(j * cap, 16), cap), :]
            gp[g * per + j, :, :cap] = dot(ones_units, p, NT, lax.Precision.HIGHEST)

        loop(per, gate_sum)
        for copy in exchange(g):
            copy.start()

        @pl.when(i > 0)
        def _():
            finish(order(i - 1 + groups))

    gp[...] = jnp.zeros_like(gp)
    loop(groups, backward)
    finish(order(groups - 1))

    acc[...] = jnp.zeros_like(acc)
    for h in range(2):
        def grads(c, h=h):
            cols = pl.ds(pl.multiple_of(c * tile, tile), tile)
            q = dot(xr[h, :, cols], gpgu[...], TN).astype(BF16)
            wg[h, cols, :] = q[:, :units]
            wu[h, cols, :] = q[:, units:]
            f = q.astype(F32)
            f = f * f
            sqs[0, h, c] = dot(ones_units, f[:, :units], NT, lax.Precision.HIGHEST)
            sqs[1, h, c] = dot(ones_units, f[:, units:], NT, lax.Precision.HIGHEST)
            d = dot(wt[...], dyr[h, :, cols], TN).astype(BF16)
            wd[:, pl.ds(pl.multiple_of(h * share + c * tile, tile), tile)] = d
            d = d.astype(F32)
            acc[...] += d * d

        loop(share // tile, grads)

    stores = [
        pltpu.make_async_copy(a, b, o_sem.at[i])
        for i, (a, b) in enumerate(((wg, ggw), (wu, guw), (wd, gdw)))
    ]
    for store in stores:
        store.start()
    squares = remote(sqs, sqr, e_sem.at[0], e_sem.at[1], tp=other)
    squares.start()
    sqd_out[...] = dot(jnp.ones((8, tile), F32), acc[...], NT, lax.Precision.HIGHEST)
    squares.wait()
    sq_out[...] = sqs[...] + sqr[...]
    for store in stores:
        store.wait()

    def drain(k):
        d = peer(k)
        for which, (src, dst) in enumerate(ins):
            remote(src.at[d], dst.at[t, rows(me)], s_sem.at[which, d],
                   r_sem.at[which, me], ep=d).wait_send()
        remote(sg.at[d], gr.at[me], gs_sem.at[d], gr_sem.at[me], ep=d).wait_send()
        for copy in back_copies(d):
            copy.wait_send()

    loop(n - 1, drain)

    def drain_pair(s):
        for which, (src, dst) in enumerate(ins):
            remote(dst.at[t, rows(s)], dst.at[t, rows(s)], fs_sem.at[which, s],
                   fr_sem.at[which, s], tp=other).wait_send()
        pltpu.make_async_copy(rg.at[rows(s)], back.at[s], br_sem.at[s]).wait()
        pltpu.make_async_copy(gt.at[s], gback.at[s], hr_sem.at[s]).wait()

    loop(n, drain_pair)

    def drain_group(g):
        for copy in exchange(g):
            copy.wait_send()

    loop(groups, drain_group)


def fused(n, cap, send_x, send_dy, send_gate, w_gate, w_up, w_down):
    width, units = w_gate.shape
    share = send_x.shape[2]
    total = n * cap
    groups = 4
    tile = 512
    any_spec = pl.BlockSpec(memory_space=pl.ANY)
    vmem = pl.BlockSpec(memory_space=pltpu.VMEM)
    sq_shape = (2, 2, share // tile, 8, tile)
    dma = pltpu.SemaphoreType.DMA
    shape = jax.ShapeDtypeStruct
    return pl.pallas_call(
        functools.partial(kernel, n, cap, units, share, groups, tile),
        out_shape=(
            shape((n, cap, share), BF16),
            shape((n, 8, 128), F32),
            shape((2, share, units), BF16),
            shape((2, share, units), BF16),
            shape((units, width), BF16),
            shape(sq_shape, F32),
            shape((8, units), F32),
        ),
        in_specs=[any_spec] * 6,
        out_specs=(any_spec,) * 5 + (vmem, vmem),
        scratch_shapes=[
            pltpu.VMEM((2, total, share), BF16),
            pltpu.VMEM((2, total, share), BF16),
            pltpu.VMEM((n, 8, 128), F32),
            pltpu.VMEM((2, share, units), BF16),
            pltpu.VMEM((2, share, units), BF16),
            pltpu.VMEM((units, width), BF16),
            pltpu.VMEM((total, units), F32),
            pltpu.VMEM((total, units), F32),
            pltpu.VMEM((total // groups, units), F32),
            pltpu.VMEM((total, 2 * units), BF16),
            pltpu.VMEM((total, units), BF16),
            pltpu.VMEM((total, share), BF16),
            pltpu.VMEM((total, share), BF16),
            pltpu.VMEM((total, share), BF16),
            pltpu.VMEM((total, share), BF16),
            pltpu.VMEM((n, 8, 128), F32),
            pltpu.VMEM((n, 8, 128), F32),
            pltpu.VMEM((n, 8, 128), F32),
            pltpu.VMEM((total, 128), F32),
            pltpu.VMEM(sq_shape, F32),
            pltpu.VMEM(sq_shape, F32),
            pltpu.VMEM((units, tile), F32),
            dma((3,)), dma((2, n)), dma((2, n)), dma((n,)), dma((n,)), dma((2, n)), dma((2, n)),
            dma((groups,)), dma((groups,)), dma((groups,)), dma((groups,)),
            dma((n,)), dma((n,)), dma((n,)), dma((n,)), dma((3,)), dma((2,)),
        ],
        compiler_params=pltpu.CompilerParams(
            collective_id=0, has_side_effects=True, vmem_limit_bytes=63 << 20
        ),
    )(send_x, send_dy, send_gate,
      w_gate.reshape(2, share, units), w_up.reshape(2, share, units), w_down)


def body(tokens, cotangent, gates, experts, gate_w, up_w, down_w):
    tok_rows, width = tokens.shape
    top_count = experts.shape[1]
    n_ep = lax.axis_size("ep")
    n_cores = lax.axis_size("tp")
    capacity = 3 * tok_rows * top_count // (2 * n_ep)
    cap = -(-capacity // 16) * 16
    n_slots = n_ep * cap
    flat_ids = experts.reshape(-1)
    onehot = (flat_ids[:, None] == jnp.arange(n_ep, dtype=jnp.int32)[None, :]).astype(jnp.int32)
    earlier = jnp.cumsum(onehot, axis=0) - onehot
    slot_of = jnp.sum(earlier * onehot, axis=1)
    target = flat_ids * cap + slot_of
    placing = (target[None, :] == jnp.arange(n_slots, dtype=jnp.int32)[:, None]).astype(F32)
    place_tok = jnp.sum(placing.reshape(n_slots, tok_rows, top_count), axis=2).astype(BF16)
    send_gate = jnp.dot(placing, gates.reshape(-1), precision=lax.Precision.HIGHEST)
    send_gate = jnp.pad(send_gate.reshape(n_ep, 1, cap), ((0, 0), (0, 7), (0, 128 - cap)))
    share = width // n_cores
    offset = lax.axis_index("tp") * share
    tok_share = lax.dynamic_slice_in_dim(tokens, offset, share, 1)
    cot_share = lax.dynamic_slice_in_dim(cotangent, offset, share, 1)
    send_x = jnp.dot(place_tok, tok_share, preferred_element_type=F32).astype(BF16)
    send_dy = jnp.dot(place_tok, cot_share, preferred_element_type=F32).astype(BF16)
    back, gback, ggw, guw, gdw, sq, sqd = fused(
        n_ep, cap, send_x.reshape(n_ep, cap, share), send_dy.reshape(n_ep, cap, share),
        send_gate, gate_w[0], up_w[0], down_w[0],
    )
    grad_tokens = lax.dot_general(
        place_tok, back.reshape(n_slots, share), TN, preferred_element_type=F32
    ).astype(BF16)
    grad_gates = jnp.dot(
        gback[:, 0, :cap].reshape(n_slots), placing, precision=lax.Precision.HIGHEST
    ).reshape(tok_rows, top_count)
    full_units = gate_w.shape[2] * n_cores
    sq = sq[:, :, :, 0, :].reshape(2, width) / full_units
    return (
        grad_tokens,
        grad_gates,
        ggw.reshape(gate_w.shape),
        guw.reshape(up_w.shape),
        gdw[None],
        sq[0][None],
        sq[1][None],
        sqd[0:1] / width,
    )


def solution(mesh):
    placed = (
        P("ep", None),
        P("ep", None),
        P("ep", None),
        P("ep", None),
        P("ep", None, "tp"),
        P("ep", None, "tp"),
        P("ep", "tp", None),
    )
    return jax.shard_map(
        body,
        mesh=mesh,
        in_specs=placed,
        out_specs=(
            P("ep", "tp"),
            P("ep", None),
            P("ep", None, "tp"),
            P("ep", None, "tp"),
            P("ep", "tp", None),
            P("ep", None),
            P("ep", None),
            P("ep", "tp"),
        ),
        check_vma=False,
    )
```

profile of v0, /device:TPU:15, one launch (start us, length us, event | category | flops | bytes accessed | tf_op | source)
XLA Modules:
  0.0 257.0 jit_solution(17131096638502251257)
XLA Ops:
  0.6 0.8 copy.32
  1.5 0.1 eq.75
  1.6 0.1 eq.79
  1.8 1.2 reduce-window.6
  2.9 0.2 slice_reduce_fusion
  3.2 0.1 fusion.15
  3.3 0.1 reduce_sum.21
  3.4 0.1 copy.35
  3.5 0.7 multiply_add_fusion.2
  4.2 0.8 copy.36
  5.0 0.1 reshape.122
  5.2 1.3 fusion.5
  6.5 0.0 copy-start.2
  6.5 0.7 pad.4.sg
  7.1 0.3 convert_reduce_fusion
  7.5 3.9 %convolution_convert_fusion = bf16[768,2048]{1,0:T(8,128)(2,1)} fusion(bf16[256,4096]{1,0:T(8,128)(2,1)} %param.8, s32[]{:T(128)S(6)} %select_n.4, bf16[768,256]{1,0:T(8,128)(2,1)S(1)} %convert_reduce_fusion), kind=kOutput, calls=%fused_computation | convolution fusion | flops 806879232 | bytes 4587524 | tf_op jit(solution)/shard_map/dot_general | solution.py:352
  11.3 0.0 copy-done.2
  11.3 2.7 %convolution_convert_fusion.1 = bf16[768,2048]{1,0:T(8,128)(2,1)} fusion(bf16[256,4096]{1,0:T(8,128)(2,1)S(1)} %copy-done.2, s32[]{:T(128)S(6)} %select_n.4, bf16[768,256]{1,0:T(8,128)(2,1)S(1)} %convert_reduce_fusion), kind=kOutput, calls=%fused_computation.1 | convolution fusion | flops 806879232 | bytes 4587524 | tf_op jit(solution)/shard_map/dot_general | solution.py:351
  14.0 225.1 %shard_map.134 = (bf16[16,48,2048]{2,1,0:T(8,128)(2,1)}, f32[16,8,128]{2,1,0:T(8,128)}, bf16[2,2048,384]{2,1,0:T(8,128)(2,1)}, bf16[2,2048,384]{2,1,0:T(8,128)(2...) custom-call(bf16[16,48,2048]{2,1,0:T(8,128)(2,1)} %bitcast.45, ...), custom_call_target="tpu_custom_call" | custom-call | tf_op jit(solution)/shard_map/pallas_call | solution.py:283
  239.1 3.9 %convolution_convert_fusion.2 = bf16[256,2048]{1,0:T(8,128)(2,1)} fusion(bf16[768,2048]{1,0:T(8,128)(2,1)} %bitcast.55, bf16[768,256]{1,0:T(8,128)(2,1)S(1)} %convert_reduce_fusion), kind=kOutput, calls=%fused_computation.2 | convolution fusion | flops 805830656 | bytes 4587520 | tf_op jit(solution)/shard_map/dot_general | solution.py:357
  242.9 1.3 slice_multiply_fusion.1
  244.2 0.9 slice_reduce_fusion.1
  245.1 0.1 reshape.124
  245.2 1.0 slice_multiply_fusion
  246.1 0.6 fusion.22
  246.8 0.8 fusion.1
  247.6 0.7 copy.38
  248.3 0.0 copy-start.1
  248.3 4.0 %copy.44 = bf16[1,4096,384]{2,1,0:T(8,128)(2,1)} copy(bf16[1,4096,384]{2,1,0:T(8,128)(2,1)} %bitcast.48) | data formatting | bytes 6291456
  252.3 0.0 copy-done.1
  252.3 0.0 copy-start
  252.3 1.7 copy.45
  254.0 1.4 copy-done
  255.3 1.7 copy.46
  (5 shorter events, 0.1 us)
Async XLA Ops:
  6.5 4.9 %copy-start.2 = (bf16[256,4096]{1,0:T(8,128)(2,1)S(1)}, bf16[256,4096]{1,0:T(8,128)(2,1)}, u32[]{:S(2)}) copy-start(bf16[256,4096]{1,0:T(8,128)(2,1)} %param.7) | copy-start | bytes 6291460
  248.3 4.0 %copy-start.1 = (bf16[2,2048,384]{2,1,0:T(8,128)(2,1)S(1)}, bf16[2,2048,384]{2,1,0:T(8,128)(2,1)}, u32[]{:S(2)}) copy-start(bf16[2,2048,384]{2,1,0:T(8,128)(2,1)} %get-tuple-element.18) | copy-start | bytes 9437188
  252.3 3.0 %copy-start = (bf16[384,4096]{1,0:T(8,128)(2,1)S(1)}, bf16[384,4096]{1,0:T(8,128)(2,1)}, u32[]{:S(2)}) copy-start(bf16[384,4096]{1,0:T(8,128)(2,1)} %get-tuple-element.19) | copy-start | bytes 9437188
where the time goes:
time: 257 us
  Pallas kernels  225 us (88%)
  local copies, waits for them, and re-layouts  14.1 us (5%)
  matrix products  12.5 us (5%)
  other arithmetic  4.58 us (2%)
    pallas_call x1, Pallas kernels, fused(): pl.pallas_call(functools.partial(kernel, n, cap, units, share, groups, ti...  225 us
    unnamed x11, local copies, waits for them, and re-layouts  10.3 us

commit v1 on v0

--- a/solution.py
+++ b/solution.py
@@ -13,6 +13,8 @@
 NN = (((1,), (0,)), ((), ()))
 NT = (((1,), (1,)), ((), ()))
 TN = (((0,), (0,)), ((), ()))
+VMEM_BYTES = 67043328
+PLANES = 4
 
 
 def dot(a, b, dims, precision=None):
@@ -327,6 +329,547 @@
       w_gate.reshape(2, share, units), w_up.reshape(2, share, units), w_down)
 
 
+def relay_kernel(
+    n, planes, cap, units, share, tile, toks, full_units,
+    tok, cot, gates, experts, wg_in, wu_in, wd_in,
+    gtok, ggate, ggw, guw, gdw, sqg, squ, sqd,
+    xd, tx, pn, near, tg, rt, pq, raw, fwd, wg, wu, wd, gs, gr, gcol, pg, pu, prod, gpgu, wt,
+    give, got, rg, gp, gpp, gt, gback, back, comb, far, gout, sqs, sqr, acc,
+    w_sem, t_sem, raw_s, raw_r, meta_s, meta_r, s_sem, r_sem, f_sem, gs_sem, gr_sem, ps_sem, pr_sem,
+    xs_sem, xr_sem, qs_sem, qr_sem, bs_sem, br_sem, cs_sem, cr_sem, hs_sem, hr_sem, o_sem, e_sem, go_sem,
+):
+    me = lax.axis_index("ep")
+    t = lax.axis_index("tp")
+    other = lax.axis_size("tp") - 1 - t
+    per = n // planes
+    half = n // 2
+    rows_g = per * cap
+    hr = half * cap
+    chunks = share // tile
+    z = me // per
+    col = me % per
+    h = z // (planes // 2)
+    oh = 1 - h
+    first = h * half
+    mine = me - first
+    own_inner, own_outer = 1 + h, (planes - 1) * h
+    far_inner, far_outer = 1 + oh, (planes - 1) * oh
+    inner = z == own_inner
+    my_relay = far_inner * per + col
+    my_q = jnp.where(inner, 1, 0)
+
+    def rows(s):
+        return pl.ds(pl.multiple_of(s * cap, 16), cap)
+
+    def cols_of(c):
+        return pl.ds(pl.multiple_of(c * tile, tile), tile)
+
+    def remote(src, dst, send, recv, **where):
+        return pltpu.make_async_remote_copy(
+            src_ref=src, dst_ref=dst, send_sem=send, recv_sem=recv,
+            device_id=where, device_id_type=MESH,
+        )
+
+    def local(src, dst, sem):
+        return pltpu.make_async_copy(src, dst, sem)
+
+    def loop(count, fn):
+        def step(i, carry):
+            fn(i)
+            return carry
+        lax.fori_loop(0, count, step, 0)
+
+    def peer(k):
+        return lax.rem(me + n // 2 + k + jnp.where(k >= n - n // 2, 1, 0), n)
+
+    barrier = pltpu.get_barrier_semaphore()
+    loop(n - 1, lambda k: pl.semaphore_signal(
+        barrier, inc=1, device_id={"ep": peer(k)}, device_id_type=MESH))
+    pl.semaphore_signal(barrier, inc=1, device_id={"tp": other}, device_id_type=MESH)
+
+    my_cols = pl.ds(pl.multiple_of(t * share, share), share)
+    ins = (tok, cot)
+    shares = [local(a.at[:, my_cols], tx.at[w], t_sem.at[w]) for w, a in enumerate(ins)]
+    loads = [
+        local(a, b, w_sem.at[i])
+        for i, (a, b) in enumerate(((wg_in, wg), (wu_in, wu), (wd_in, wd)))
+    ]
+    for copy in shares:
+        copy.start()
+
+    e0, e1 = experts[0:1, :], experts[1:2, :]
+    which_expert = lax.broadcasted_iota(jnp.int32, (n, toks), 0)
+    hit0 = (which_expert == e0).astype(F32)
+    hit1 = (which_expert == e1).astype(F32)
+    before = (
+        lax.broadcasted_iota(jnp.int32, (toks, toks), 0)
+        < lax.broadcasted_iota(jnp.int32, (toks, toks), 1)
+    ).astype(F32).astype(BF16)
+    earlier = dot((hit0 + hit1).astype(BF16), before, NN)
+    t0 = e0.astype(F32) * cap + jnp.sum(earlier * hit0, axis=0, keepdims=True)
+    t1 = e1.astype(F32) * cap + jnp.sum(earlier * hit1, axis=0, keepdims=True)
+    tg[0:1, :] = t0
+    tg[1:2, :] = t1
+    tg[2:4, :] = gates[...]
+    tg[4:8, :] = jnp.zeros((4, toks), F32)
+
+    half_rows = (lax.broadcasted_iota(jnp.int32, (hr, toks), 0) + first * cap).astype(F32)
+
+    def placing(a, b):
+        return jnp.where((half_rows == a) | (half_rows == b), 1.0, 0.0).astype(BF16)
+
+    pn[...] = placing(t0, t1)
+
+    pl.semaphore_wait(barrier, n)
+
+    def raw_copy(which, c):
+        at = pl.ds(pl.multiple_of(t * share + c * tile, tile), tile)
+        return remote(ins[which].at[:, at], raw.at[my_q, which, :, cols_of(c)],
+                      raw_s.at[which, c], raw_r.at[my_q, which, c], ep=my_relay)
+
+    def raw_send():
+        for which in range(2):
+            loop(chunks, lambda c, which=which: raw_copy(which, c).start())
+
+    meta = remote(tg, rt.at[my_q], meta_s.at[0], meta_r.at[my_q], ep=my_relay)
+    meta.start()
+
+    @pl.when(z == own_outer)
+    def _():
+        raw_send()
+
+    def near_slot(k):
+        return lax.rem(mine + per + k, half)
+
+    def near_copy(which, d):
+        return remote(near.at[which, rows(d)], xd.at[which, t, rows(me)], s_sem.at[which, d],
+                      r_sem.at[which, me], ep=first + d)
+
+    for which in range(2):
+        shares[which].wait()
+
+        def place(c, which=which):
+            near[which, :, cols_of(c)] = dot(pn[...], tx[which, :, cols_of(c)], NN).astype(BF16)
+
+        loop(chunks, place)
+
+        def send(k, which=which):
+            d = near_slot(k)
+
+            @pl.when(d != mine)
+            def _():
+                near_copy(which, d).start()
+
+            @pl.when(d == mine)
+            def _():
+                local(near.at[which, rows(d)], xd.at[which, t, rows(me)], r_sem.at[which, me]).start()
+
+        loop(half, send)
+
+    for load in loads:
+        load.start()
+
+    columns = jnp.transpose(tg[...])
+    c0, c1, g0, g1 = (columns[:, i:i + 1] for i in range(4))
+    lanes = lax.broadcasted_iota(jnp.int32, (toks, 128), 1)
+    lanes = jnp.where(lanes < cap, lanes, -2 * n * cap).astype(F32)
+
+    def gate_row(e):
+        base = (e * cap).astype(F32)
+        picked = jnp.where(c0 - base == lanes, g0, 0.0) + jnp.where(c1 - base == lanes, g1, 0.0)
+        gs[e] = jnp.broadcast_to(jnp.sum(picked, axis=0, keepdims=True), (8, 128))
+
+    loop(n, gate_row)
+
+    def gate_copy(d):
+        return remote(gs.at[d], gr.at[me], gs_sem.at[d], gr_sem.at[me], ep=d)
+
+    loop(n - 1, lambda k: gate_copy(peer(k)).start())
+    local(gs.at[me], gr.at[me], gr_sem.at[me]).start()
+
+    def source_of(q):
+        return jnp.where(q == 0, far_outer, far_inner) * per + col
+
+    def fwd_copy(q, which, d, at):
+        src = source_of(q)
+        return remote(fwd.at[q, which, rows(d), at], xd.at[which, t, rows(src), at],
+                      f_sem.at[q, which, d], r_sem.at[which, src], ep=first + d)
+
+    def relay(q):
+        src = source_of(q)
+        remote(tg, rt.at[q], meta_s.at[0], meta_r.at[q], ep=my_relay).wait_recv()
+        pq[q] = placing(rt[q, 0:1, :], rt[q, 1:2, :])
+
+        def step(i):
+            which = i // chunks
+            c = i % chunks
+            at = cols_of(c)
+            remote(raw.at[q, which, :, at], raw.at[q, which, :, at], raw_s.at[0, 0],
+                   raw_r.at[q, which, c], ep=my_relay).wait_recv()
+
+            @pl.when((q == 0) & (i == 2 * chunks - 2))
+            def _():
+                raw_send()
+
+            fwd[q, which, :, at] = dot(pq[q], raw[q, which, :, at], NN).astype(BF16)
+
+            def pass_on(k):
+                d = near_slot(k)
+
+                @pl.when(d != mine)
+                def _():
+                    fwd_copy(q, which, d, at).start()
+
+                @pl.when(d == mine)
+                def _():
+                    local(fwd.at[q, which, rows(d), at], xd.at[which, t, rows(src), at],
+                          r_sem.at[which, src]).start()
+
+            loop(half, pass_on)
+
+        loop(2 * chunks, step)
+
+    def pair_copy(which, s):
+        block = xd.at[which, t, rows(s)]
+        return remote(block, block, ps_sem.at[which, s], pr_sem.at[which, s], tp=other)
+
+    def arrive(g):
+        for which in range(2):
+            def pass_on(j, which=which):
+                s = g * per + j
+                local(near.at[which, rows(0)], xd.at[which, t, rows(s)], r_sem.at[which, s]).wait()
+                pair_copy(which, s).start()
+
+            loop(per, pass_on)
+        for which in range(2):
+            def joined(j, which=which):
+                s = g * per + j
+                block = xd.at[which, other, rows(s)]
+                remote(block, block, ps_sem.at[which, s], pr_sem.at[which, s], tp=other).wait_recv()
+
+            loop(per, joined)
+
+    ones_units = jnp.ones((8, units), F32)
+
+    def exchange(g, c):
+        block = (pl.ds(pl.multiple_of(g * rows_g, 16), rows_g), cols_of(c))
+        return remote(give.at[block], got.at[block], xs_sem.at[g, c], xr_sem.at[g, c], tp=other)
+
+    def gate_exchange(g):
+        grp = pl.ds(g * per, per)
+        return remote(gp.at[grp], gpp.at[grp], qs_sem.at[g], qr_sem.at[g], tp=other)
+
+    def back_target(s):
+        g = s // per
+        close = g // (planes // 2) == h
+        dest = jnp.where(close, s, own_inner * per + s % per)
+        slot = jnp.where(close, 2, jnp.where(g == far_outer, 0, 1))
+        return dest, slot
+
+    def back_copy(s, c, at):
+        dest, slot = back_target(s)
+        return remote(rg.at[rows(s), at], back.at[slot, rows(mine), at], bs_sem.at[s],
+                      br_sem.at[slot, c], ep=dest)
+
+    def gate_back(s):
+        return remote(gt.at[s], gback.at[me], hs_sem.at[s], hr_sem.at[me], ep=s)
+
+    def group(g):
+        arrive(g)
+        r = pl.ds(pl.multiple_of(g * rows_g, 16), rows_g)
+        pg[...] = dot(xd[0, 0, r, :], wg[0], NN) + dot(xd[0, 1, r, :], wg[1], NN)
+        pu[...] = dot(xd[0, 0, r, :], wu[0], NN) + dot(xd[0, 1, r, :], wu[1], NN)
+
+        def gates_in(j):
+            s = g * per + j
+            local(gs.at[0], gr.at[s], gr_sem.at[s]).wait()
+            column = jnp.transpose(gr[s])
+            gcol[rows(j), :] = jnp.broadcast_to(column[:cap, 0:1], (cap, 128))
+
+        loop(per, gates_in)
+        dh = dot(xd[1, 0, r, :], wd[:, :share], NT) + dot(xd[1, 1, r, :], wd[:, share:], NT)
+        a = pg[...]
+        b = pu[...]
+        gate = gcol[:, 0:1]
+        sig = jax.nn.sigmoid(a)
+        silu = a * sig
+        hidden = (silu * b).astype(BF16).astype(F32)
+        prod[...] = hidden * dh
+        scaled = gate * dh
+        gpgu[r, :units] = (scaled * b * sig * (1.0 + a * (1.0 - sig))).astype(BF16)
+        gpgu[r, units:] = (scaled * silu).astype(BF16)
+        wt[r, :] = (gate * hidden).astype(BF16)
+
+        def part(c):
+            at = cols_of(c)
+            for side, dst in ((other, give), (t, rg)):
+                dst[r, at] = (
+                    dot(gpgu[r, :units], wg[side, at, :], NT)
+                    + dot(gpgu[r, units:], wu[side, at, :], NT)
+                ).astype(BF16)
+            exchange(g, c).start()
+
+        def gate_sum(j):
+            p = prod[rows(j), :]
+            gp[g * per + j, :, :cap] = dot(ones_units, p, NT, lax.Precision.HIGHEST)
+
+        def finish(c):
+            at = cols_of(c)
+            exchange(g, c).wait_recv()
+            rg[r, at] = (rg[r, at].astype(F32) + got[r, at].astype(F32)).astype(BF16)
+
+            def out(j):
+                s = g * per + j
+                dest, slot = back_target(s)
+
+                @pl.when(dest == me)
+                def _():
+                    local(rg.at[rows(s), at], back.at[slot, rows(mine), at],
+                          br_sem.at[slot, c]).start()
+
+                @pl.when(dest != me)
+                def _():
+                    back_copy(s, c, at).start()
+
+            loop(per, out)
+
+        def column(c):
+            @pl.when(c < chunks)
+            def _():
+                part(c)
+
+            @pl.when(c > 0)
+            def _():
+                finish(c - 1)
+
+        loop(chunks + 1, column)
+        loop(per, gate_sum)
+        gate_exchange(g).start()
+        gate_exchange(g).wait_recv()
+
+        def gates_out(j):
+            s = g * per + j
+            gt[s] = gp[s] + gpp[s]
+
+            @pl.when(s == me)
+            def _():
+                local(gt.at[s], gback.at[me], hr_sem.at[me]).start()
+
+            @pl.when(s != me)
+            def _():
+                gate_back(s).start()
+
+        loop(per, gates_out)
+
+    def comb_copy(q, at, c):
+        return remote(comb.at[q, :, at], far.at[:, at], cs_sem.at[q, c], cr_sem.at[c],
+                      ep=source_of(q))
+
+    def combine(q, c):
+        at = cols_of(c)
+        local(near.at[0, :, at], back.at[q, :, at], br_sem.at[q, c]).wait()
+        comb[q, :, at] = dot(pq[q], back[q, :, at], TN).astype(BF16)
+        comb_copy(q, at, c).start()
+
+    gp[...] = jnp.zeros_like(gp)
+    for load in loads:
+        load.wait()
+
+    def phase(i):
+        @pl.when(inner & (i % 2 == 0))
+        def _():
+            relay(i // 2)
+
+        @pl.when(inner & (i == planes - 1))
+        def _():
+            loop(chunks, lambda c: combine(0, c))
+
+        on_inner = jnp.where(i == 1, far_outer, jnp.where(i == 2, far_inner, own_outer))
+        on_outer = jnp.where(i == 1, own_inner, jnp.where(i == 2, far_outer, far_inner))
+        group(jnp.where(i == 0, z, jnp.where(inner, on_inner, on_outer)))
+
+    loop(planes, phase)
+
+    acc[...] = jnp.zeros_like(acc)
+
+    def grads(i):
+        side = i // chunks
+        at = cols_of(i % chunks)
+        wide = cols_of(i)
+        q = dot(xd[0, side, :, at], gpgu[...], TN).astype(BF16)
+        wg[side, at, :] = q[:, :units]
+        wu[side, at, :] = q[:, units:]
+        f = q.astype(F32)
+        f = f * f
+        sqs[0, :, wide] = dot(ones_units, f[:, :units], NT, lax.Precision.HIGHEST)
+        sqs[1, :, wide] = dot(ones_units, f[:, units:], NT, lax.Precision.HIGHEST)
+        d = dot(wt[...], xd[1, side, :, at], TN).astype(BF16)
+        wd[:, wide] = d
+        d = d.astype(F32)
+        acc[...] += d * d
+
+        @pl.when(inner & (i % 2 == 1))
+        def _():
+            combine(1, i // 2)
+
+    loop(2 * chunks, grads)
+
+    stores = [
+        local(a, b, o_sem.at[i])
+        for i, (a, b) in enumerate(((wg, ggw), (wu, guw), (wd, gdw)))
+    ]
+    for store in stores:
+        store.start()
+    squares = remote(sqs, sqr, e_sem.at[0], e_sem.at[1], tp=other)
+    squares.start()
+    sum_down = dot(jnp.ones((8, tile), F32), acc[...], NT, lax.Precision.HIGHEST)
+    sqd[...] = sum_down[0:1, :] / (2 * share)
+    squares.wait()
+    sqg[...] = (sqs[0, 0:1, :] + sqr[0, 0:1, :]) / full_units
+    squ[...] = (sqs[1, 0:1, :] + sqr[1, 0:1, :]) / full_units
+
+    loop(n, lambda e: local(gt.at[e], gback.at[e], hr_sem.at[e]).wait())
+    slots = lax.broadcasted_iota(jnp.int32, (cap, toks), 0)
+
+    def look_up(e, carry):
+        column = jnp.transpose(gback[e])[:cap, 0:1]
+        at = (slots + e * cap).astype(F32)
+        return tuple(
+            v + jnp.where(at == tg[k:k + 1, :], column, 0.0) for k, v in enumerate(carry)
+        )
+
+    zero = jnp.zeros((cap, toks), F32)
+    found = lax.fori_loop(0, n, look_up, (zero, zero))
+    for k in range(2):
+        ggate[k:k + 1, :] = jnp.sum(found[k], axis=0, keepdims=True)
+
+    def last(c):
+        at = cols_of(c)
+        local(near.at[0, :, at], back.at[2, :, at], br_sem.at[2, c]).wait()
+        close = dot(pn[...], back[2, :, at], TN)
+        local(far.at[:, at], far.at[:, at], cr_sem.at[c]).wait()
+        gout[:, at] = (close + far[:, at].astype(F32)).astype(BF16)
+        local(gout.at[:, at], gtok.at[:, at], go_sem.at[c]).start()
+
+    loop(chunks, last)
+
+    for store in stores:
+        store.wait()
+    loop(chunks, lambda c: local(gout.at[:, cols_of(c)], gtok.at[:, cols_of(c)], go_sem.at[c]).wait())
+
+    meta.wait_send()
+    for which in range(2):
+        loop(chunks, lambda c, which=which: raw_copy(which, c).wait_send())
+
+    def drain_near(d):
+        @pl.when(d != mine)
+        def _():
+            for which in range(2):
+                near_copy(which, d).wait_send()
+
+            @pl.when(inner)
+            def _():
+                for q in range(2):
+                    for which in range(2):
+                        fwd_copy(q, which, d, pl.ds(0, share)).wait_send()
+
+    loop(half, drain_near)
+
+    def drain(k):
+        d = peer(k)
+        gate_copy(d).wait_send()
+        gate_back(d).wait_send()
+
+    loop(n - 1, drain)
+
+    def drain_rows(s):
+        for which in range(2):
+            pair_copy(which, s).wait_send()
+        dest, _ = back_target(s)
+
+        @pl.when(dest != me)
+        def _():
+            back_copy(s, 0, pl.ds(0, share)).wait_send()
+
+    loop(n, drain_rows)
+
+    def drain_group(g):
+        loop(chunks, lambda c: exchange(g, c).wait_send())
+        gate_exchange(g).wait_send()
+
+    loop(planes, drain_group)
+
+    @pl.when(inner)
+    def _():
+        for q in range(2):
+            loop(chunks, lambda c, q=q: comb_copy(q, cols_of(c), c).wait_send())
+
+
+def relay_scratch(n, planes, cap, units, share, tile, toks):
+    total = n * cap
+    group = total // planes
+    hr = n // 2 * cap
+    chunks = share // tile
+    half = n // 2
+    width = 2 * share
+    arrays = [
+        ((2, 2, total, share), BF16), ((2, toks, share), BF16), ((hr, toks), BF16),
+        ((2, hr, share), BF16), ((8, toks), F32), ((2, 8, toks), F32), ((2, hr, toks), BF16),
+        ((2, 2, toks, share), BF16), ((2, 2, hr, share), BF16),
+        ((2, share, units), BF16), ((2, share, units), BF16), ((units, width), BF16),
+        ((n, 8, 128), F32), ((n, 8, 128), F32), ((group, 128), F32),
+        ((group, units), F32), ((group, units), F32), ((group, units), F32),
+        ((total, 2 * units), BF16), ((total, units), BF16),
+        ((total, share), BF16), ((total, share), BF16), ((total, share), BF16),
+        ((n, 8, 128), F32), ((n, 8, 128), F32), ((n, 8, 128), F32), ((n, 8, 128), F32),
+        ((3, hr, share), BF16), ((2, toks, share), BF16), ((toks, share), BF16),
+        ((toks, share), BF16), ((2, 8, width), F32), ((2, 8, width), F32), ((units, tile), F32),
+    ]
+    sems = [
+        (3,), (2,), (2, chunks), (2, 2, chunks), (1,), (2,), (2, half), (2, n), (2, 2, half),
+        (n,), (n,), (2, n), (2, n), (planes, chunks), (planes, chunks), (planes,), (planes,),
+        (n,), (3, chunks), (2, chunks), (chunks,), (n,), (n,), (3,), (2,), (chunks,),
+    ]
+    size = 0
+    for dims, kind in arrays:
+        count = jnp.dtype(kind).itemsize
+        for d in dims:
+            count *= d
+        size += count
+    return arrays, sems, size
+
+
+def fused_relay(n, planes, cap, toks, tile, tokens, cotangent, gates, experts, w_gate, w_up, w_down):
+    width, units = w_gate.shape
+    cores = lax.axis_size("tp")
+    share = width // cores
+    any_spec = pl.BlockSpec(memory_space=pl.ANY)
+    vmem = pl.BlockSpec(memory_space=pltpu.VMEM)
+    shape = jax.ShapeDtypeStruct
+    arrays, sems, _ = relay_scratch(n, planes, cap, units, share, tile, toks)
+    return pl.pallas_call(
+        functools.partial(relay_kernel, n, planes, cap, units, share, tile, toks, units * cores),
+        out_shape=(
+            shape((toks, share), BF16),
+            shape((2, toks), F32),
+            shape((2, share, units), BF16),
+            shape((2, share, units), BF16),
+            shape((units, width), BF16),
+            shape((1, width), F32),
+            shape((1, width), F32),
+            shape((1, units), F32),
+        ),
+        in_specs=[any_spec, any_spec, vmem, vmem, any_spec, any_spec, any_spec],
+        out_specs=(any_spec, vmem, any_spec, any_spec, any_spec, vmem, vmem, vmem),
+        scratch_shapes=[pltpu.VMEM(dims, kind) for dims, kind in arrays]
+        + [pltpu.SemaphoreType.DMA(dims) for dims in sems],
+        compiler_params=pltpu.CompilerParams(
+            collective_id=0, has_side_effects=True, vmem_limit_bytes=VMEM_BYTES
+        ),
+    )(tokens, cotangent, gates.T, experts.T,
+      w_gate.reshape(2, share, units), w_up.reshape(2, share, units), w_down)
+
+
 def body(tokens, cotangent, gates, experts, gate_w, up_w, down_w):
     tok_rows, width = tokens.shape
     top_count = experts.shape[1]
@@ -335,6 +878,19 @@
     capacity = 3 * tok_rows * top_count // (2 * n_ep)
     cap = -(-capacity // 16) * 16
     n_slots = n_ep * cap
+    share = width // n_cores
+    tile = 512
+    units = gate_w.shape[2]
+    _, _, size = relay_scratch(n_ep, PLANES, cap, units, share, tile, tok_rows)
+    if n_ep % PLANES == 0 and tok_rows < n_ep // 2 * cap and size + (3 << 20) < VMEM_BYTES:
+        gtok, ggate, ggw, guw, gdw, sqg, squ, sqd = fused_relay(
+            n_ep, PLANES, cap, tok_rows, tile, tokens, cotangent, gates, experts,
+            gate_w[0], up_w[0], down_w[0],
+        )
+        return (
+            gtok, ggate.T, ggw.reshape(gate_w.shape), guw.reshape(up_w.shape), gdw[None],
+            sqg, squ, sqd,
+        )
     flat_ids = experts.reshape(-1)
     onehot = (flat_ids[:, None] == jnp.arange(n_ep, dtype=jnp.int32)[None, :]).astype(jnp.int32)
     earlier = jnp.cumsum(onehot, axis=0) - onehot

time: 257 us -> 216 us (0.84)
  Pallas kernels: 225 us -> 199 us
  matrix products: 12.5 us -> 0 us
  other arithmetic: 4.58 us -> 0 us
    pallas_call x1, Pallas kernels: 225 us -> 199 us  [fused_relay(): pl.pallas_call(functools.partial(relay_kernel, n, planes, cap, units, sha...]
    dot_general x5 -> x0, matrix products: 12.5 us -> none  [the longest x1 3.89 us: body(): jnp.dot(place_tok, cot_share, preferred_element_type=F32).astype(BF16)]
    unnamed x11 -> x18, local copies, waits for them, and re-layouts: 10.3 us -> 14.1 us
where the time goes in v1:
time: 216 us; the launch traced here: 214 us
  Pallas kernels  199 us (92%)
  local copies, waits for them, and re-layouts  14.1 us (7%)
    pallas_call x1, Pallas kernels, fused_relay(): pl.pallas_call(functools.partial(relay_kernel, n, planes, cap, units, sha...  199 us
    unnamed x18, local copies, waits for them, and re-layouts  14.1 us

profile of v1, /device:TPU:15, one launch (start us, length us, event | category | flops | bytes accessed | tf_op | source)
XLA Modules:
  0.0 214.1 jit_solution(14852376595288301473)
XLA Ops:
  0.6 199.4 %shard_map.134 = (bf16[256,2048]{1,0:T(8,128)(2,1)}, f32[2,256]{1,0:T(2,128)}, bf16[2,2048,384]{2,1,0:T(8,128)(2,1)}, bf16[2,2048,384]{2,1,0:T(8,128)(2,1)}, bf1...) custom-call(bf16[256,4096]{1,0:T(8,128)(2,1)} %tok.1, ...), custom_call_target="tpu_custom_call" | custom-call | tf_op jit(solution)/shard_map/pallas_call | solution.py:850
  200.0 2.3 %copy.23 = bf16[256,2048]{1,0:T(8,128)(2,1)} copy(bf16[256,2048]{1,0:T(8,128)(2,1)} %get-tuple-element.32) | data formatting | bytes 2097152
  202.3 1.3 copy.24
  203.6 0.0 copy-start.1
  203.6 4.0 %copy.25 = bf16[1,4096,384]{2,1,0:T(8,128)(2,1)} copy(bf16[1,4096,384]{2,1,0:T(8,128)(2,1)} %bitcast.11) | data formatting | bytes 6291456
  207.6 0.0 copy-done.1
  207.6 0.0 copy-start
  207.6 1.7 copy.26
  209.3 1.4 copy-done
  210.7 0.0 copy-start.3
  210.7 0.0 copy-start.2
  210.7 0.0 copy-start.4
  210.7 1.7 copy.27
  212.3 0.0 copy-done.3
  212.3 0.6 copy.28
  212.9 0.0 copy-done.2
  212.9 0.6 copy.29
  213.5 0.0 copy-done.4
  213.5 0.6 copy.30
Async XLA Ops:
  203.6 4.0 %copy-start.1 = (bf16[2,2048,384]{2,1,0:T(8,128)(2,1)S(1)}, bf16[2,2048,384]{2,1,0:T(8,128)(2,1)}, u32[]{:S(2)}) copy-start(bf16[2,2048,384]{2,1,0:T(8,128)(2,1)} %get-tuple-element.19) | copy-start | bytes 9437188
  207.6 3.0 %copy-start = (bf16[384,4096]{1,0:T(8,128)(2,1)S(1)}, bf16[384,4096]{1,0:T(8,128)(2,1)}, u32[]{:S(2)}) copy-start(bf16[384,4096]{1,0:T(8,128)(2,1)} %get-tuple-element.20) | copy-start | bytes 9437188
  210.7 1.7 copy-start.3
  210.7 2.3 %copy-start.2 = (f32[1,4096]{1,0:T(1,128)S(1)}, f32[1,4096]{1,0:T(1,128)}, u32[]{:S(2)}) copy-start(f32[1,4096]{1,0:T(1,128)} %get-tuple-element.38) | copy-start | bytes 49156
  210.7 2.9 %copy-start.4 = (f32[1,384]{1,0:T(1,128)S(1)}, f32[1,384]{1,0:T(1,128)}, u32[]{:S(2)}) copy-start(f32[1,384]{1,0:T(1,128)} %get-tuple-element.39) | copy-start | bytes 4612

commit v2 on v1

--- a/solution.py
+++ b/solution.py
@@ -334,9 +334,10 @@
     tok, cot, gates, experts, wg_in, wu_in, wd_in,
     gtok, ggate, ggw, guw, gdw, sqg, squ, sqd,
     xd, tx, pn, near, tg, rt, pq, raw, fwd, wg, wu, wd, gs, gr, gcol, pg, pu, prod, gpgu, wt,
-    give, got, rg, gp, gpp, gt, gback, back, comb, far, gout, sqs, sqr, acc,
+    give, got, rg, gp, gpp, gt, gback, back, comb, far, mid, pm, sqs, sqr, acc,
     w_sem, t_sem, raw_s, raw_r, meta_s, meta_r, s_sem, r_sem, f_sem, gs_sem, gr_sem, ps_sem, pr_sem,
     xs_sem, xr_sem, qs_sem, qr_sem, bs_sem, br_sem, cs_sem, cr_sem, hs_sem, hr_sem, o_sem, e_sem, go_sem,
+    n_sem, ms_sem, mr_sem, bf_sem, bg_sem,
 ):
     me = lax.axis_index("ep")
     t = lax.axis_index("tp")
@@ -355,6 +356,8 @@
     own_inner, own_outer = 1 + h, (planes - 1) * h
     far_inner, far_outer = 1 + oh, (planes - 1) * oh
     inner = z == own_inner
+    outer = z == own_outer
+    next_plane = own_inner + own_outer - z
     my_relay = far_inner * per + col
     my_q = jnp.where(inner, 1, 0)
 
@@ -420,6 +423,18 @@
 
     pn[...] = placing(t0, t1)
 
+    columns = jnp.transpose(tg[...])
+    c0, c1, g0, g1 = (columns[:, i:i + 1] for i in range(4))
+    lanes = lax.broadcasted_iota(jnp.int32, (toks, 128), 1)
+    lanes = jnp.where(lanes < cap, lanes, -2 * n * cap).astype(F32)
+
+    def gate_row(e):
+        base = (e * cap).astype(F32)
+        picked = jnp.where(c0 - base == lanes, g0, 0.0) + jnp.where(c1 - base == lanes, g1, 0.0)
+        gs[e, 0:1, :] = jnp.sum(picked, axis=0, keepdims=True)
+
+    loop(n, gate_row)
+
     pl.semaphore_wait(barrier, n)
 
     def raw_copy(which, c):
@@ -431,76 +446,117 @@
         for which in range(2):
             loop(chunks, lambda c, which=which: raw_copy(which, c).start())
 
+    first_row = pl.ds(0, 1)
+
+    def gate_copy(d):
+        return remote(gs.at[d, first_row], gr.at[me, first_row], gs_sem.at[d], gr_sem.at[me], ep=d)
+
+    loop(n - 1, lambda k: gate_copy(peer(k)).start())
+    local(gs.at[me, first_row], gr.at[me, first_row], gr_sem.at[me]).start()
+
     meta = remote(tg, rt.at[my_q], meta_s.at[0], meta_r.at[my_q], ep=my_relay)
     meta.start()
-
-    @pl.when(z == own_outer)
+    close_meta = remote(tg, rt.at[2], meta_s.at[1], meta_r.at[2], ep=own_inner * per + col)
+
+    @pl.when(outer)
+    def _():
+        close_meta.start()
+
+    @pl.when(outer)
     def _():
         raw_send()
 
-    def near_slot(k):
-        return lax.rem(mine + per + k, half)
-
-    def near_copy(which, d):
-        return remote(near.at[which, rows(d)], xd.at[which, t, rows(me)], s_sem.at[which, d],
-                      r_sem.at[which, me], ep=first + d)
-
-    for which in range(2):
+    def near_copy(which, j):
+        return remote(near.at[which, rows(z * per - first + j)], xd.at[which, t, rows(me)],
+                      s_sem.at[which, j], r_sem.at[which, me], ep=z * per + j)
+
+    def next_copy(which, c, at):
+        return remote(near.at[which, next_block, at], raw.at[2, which, block, at],
+                      n_sem.at[which], raw_r.at[2, which, c], ep=next_plane * per + col)
+
+    def next_send(which):
+        loop(chunks, lambda c: next_copy(which, c, cols_of(c)).start())
+
+    next_block = pl.ds(pl.multiple_of((next_plane * per - first) * cap, 16), rows_g)
+    own_block = pl.ds(pl.multiple_of((z * per - first) * cap, 16), rows_g)
+    block = pl.ds(0, rows_g)
+
+    def near_send(which):
         shares[which].wait()
 
-        def place(c, which=which):
+        def place(c):
             near[which, :, cols_of(c)] = dot(pn[...], tx[which, :, cols_of(c)], NN).astype(BF16)
 
         loop(chunks, place)
 
-        def send(k, which=which):
-            d = near_slot(k)
-
-            @pl.when(d != mine)
-            def _():
-                near_copy(which, d).start()
-
-            @pl.when(d == mine)
-            def _():
-                local(near.at[which, rows(d)], xd.at[which, t, rows(me)], r_sem.at[which, me]).start()
-
-        loop(half, send)
+        def send(k):
+            j = lax.rem(col + 1 + k, per)
+
+            @pl.when(j != col)
+            def _():
+                near_copy(which, j).start()
+
+            @pl.when(j == col)
+            def _():
+                local(near.at[which, rows(mine)], xd.at[which, t, rows(me)], r_sem.at[which, me]).start()
+
+        loop(per, send)
+
+    near_send(0)
+    next_send(0)
+    near_send(1)
 
     for load in loads:
         load.start()
 
-    columns = jnp.transpose(tg[...])
-    c0, c1, g0, g1 = (columns[:, i:i + 1] for i in range(4))
-    lanes = lax.broadcasted_iota(jnp.int32, (toks, 128), 1)
-    lanes = jnp.where(lanes < cap, lanes, -2 * n * cap).astype(F32)
-
-    def gate_row(e):
-        base = (e * cap).astype(F32)
-        picked = jnp.where(c0 - base == lanes, g0, 0.0) + jnp.where(c1 - base == lanes, g1, 0.0)
-        gs[e] = jnp.broadcast_to(jnp.sum(picked, axis=0, keepdims=True), (8, 128))
-
-    loop(n, gate_row)
-
-    def gate_copy(d):
-        return remote(gs.at[d], gr.at[me], gs_sem.at[d], gr_sem.at[me], ep=d)
-
-    loop(n - 1, lambda k: gate_copy(peer(k)).start())
-    local(gs.at[me], gr.at[me], gr_sem.at[me]).start()
-
     def source_of(q):
-        return jnp.where(q == 0, far_outer, far_inner) * per + col
-
-    def fwd_copy(q, which, d, at):
+        return jnp.where(q == 0, far_outer, jnp.where(q == 1, far_inner, next_plane)) * per + col
+
+    def cross_copy(q, which, c, at):
+        return remote(fwd.at[q, which, next_block, at], raw.at[q, which, block, at],
+                      f_sem.at[q, which, col], raw_r.at[q, which, c], ep=own_outer * per + col)
+
+    def spread_copy(src_rows, q, which, j, at):
         src = source_of(q)
-        return remote(fwd.at[q, which, rows(d), at], xd.at[which, t, rows(src), at],
-                      f_sem.at[q, which, d], r_sem.at[which, src], ep=first + d)
-
-    def relay(q):
+        return remote(src_rows, xd.at[which, t, rows(src), at],
+                      f_sem.at[q, which, j], r_sem.at[which, src], ep=z * per + j)
+
+    def spread(buf, base, q, which, at):
         src = source_of(q)
+
+        def one(k):
+            j = lax.rem(col + 1 + k, per)
+            src_rows = buf.at[q, which, rows(base + j), at]
+
+            @pl.when(j != col)
+            def _():
+                spread_copy(src_rows, q, which, j, at).start()
+
+            @pl.when(j == col)
+            def _():
+                local(src_rows, xd.at[which, t, rows(src), at], r_sem.at[which, src]).start()
+
+        loop(per, one)
+
+    def scatter(q, begin, count):
+        def step(k):
+            i = begin + k
+            which = i // chunks
+            c = i % chunks
+            at = cols_of(c)
+            part = raw.at[q, which, block, at]
+            remote(part, part, raw_s.at[0, 0], raw_r.at[q, which, c], ep=my_relay).wait_recv()
+            spread(raw, 0, q, which, at)
+
+        loop(count, step)
+
+    def relay_start(q):
         remote(tg, rt.at[q], meta_s.at[0], meta_r.at[q], ep=my_relay).wait_recv()
         pq[q] = placing(rt[q, 0:1, :], rt[q, 1:2, :])
 
-        def step(i):
+    def relay(q, begin, count):
+        def step(k):
+            i = begin + k
             which = i // chunks
             c = i % chunks
             at = cols_of(c)
@@ -513,21 +569,10 @@
 
             fwd[q, which, :, at] = dot(pq[q], raw[q, which, :, at], NN).astype(BF16)
 
-            def pass_on(k):
-                d = near_slot(k)
-
-                @pl.when(d != mine)
-                def _():
-                    fwd_copy(q, which, d, at).start()
-
-                @pl.when(d == mine)
-                def _():
-                    local(fwd.at[q, which, rows(d), at], xd.at[which, t, rows(src), at],
-                          r_sem.at[which, src]).start()
-
-            loop(half, pass_on)
-
-        loop(2 * chunks, step)
+            cross_copy(q, which, c, at).start()
+            spread(fwd, own_inner * per - first, q, which, at)
+
+        loop(count, step)
 
     def pair_copy(which, s):
         block = xd.at[which, t, rows(s)]
@@ -549,32 +594,67 @@
 
             loop(per, joined)
 
-    ones_units = jnp.ones((8, units), F32)
-
-    def exchange(g, c):
-        block = (pl.ds(pl.multiple_of(g * rows_g, 16), rows_g), cols_of(c))
-        return remote(give.at[block], got.at[block], xs_sem.at[g, c], xr_sem.at[g, c], tp=other)
+    def lane_sums(v):
+        ones = jnp.ones((8, v.shape[1]), BF16)
+        high = v.astype(BF16)
+        low = (v - high.astype(F32)).astype(BF16)
+        return dot(ones, high, NT) + dot(ones, low, NT)
+
+    def exchange(i, c):
+        at = cols_of(c)
+        return remote(give.at[i % 2, :, at], got.at[i % 2, :, at], xs_sem.at[i, c],
+                      xr_sem.at[i, c], tp=other)
 
     def gate_exchange(g):
         grp = pl.ds(g * per, per)
         return remote(gp.at[grp], gpp.at[grp], qs_sem.at[g], qr_sem.at[g], tp=other)
 
-    def back_target(s):
-        g = s // per
-        close = g // (planes // 2) == h
-        dest = jnp.where(close, s, own_inner * per + s % per)
-        slot = jnp.where(close, 2, jnp.where(g == far_outer, 0, 1))
-        return dest, slot
+    def back_slot(g):
+        far_slot = jnp.where(g == far_outer, 0, 1)
+        return jnp.where(g == z, 2, jnp.where(g == next_plane, 3, far_slot))
 
     def back_copy(s, c, at):
-        dest, slot = back_target(s)
+        slot = back_slot(s // per)
         return remote(rg.at[rows(s), at], back.at[slot, rows(mine), at], bs_sem.at[s],
-                      br_sem.at[slot, c], ep=dest)
+                      br_sem.at[slot, c], ep=z * per + s % per)
+
+    def gathered(slot, c, at, sem):
+        local(near.at[0, block, at], back.at[slot, block, at], sem.at[slot, c]).wait()
+
+    def up_copy(slot, c, at):
+        to = jnp.where(slot == 3, 2, slot)
+        return remote(back.at[slot, own_block, at], back.at[to, own_block, at],
+                      bf_sem.at[slot], bg_sem.at[to, c], ep=own_inner * per + col)
+
+    def up(slot):
+        def step(c):
+            at = cols_of(c)
+            gathered(slot, c, at, br_sem)
+            up_copy(slot, c, at).start()
+
+        loop(chunks, step)
 
     def gate_back(s):
-        return remote(gt.at[s], gback.at[me], hs_sem.at[s], hr_sem.at[me], ep=s)
-
-    def group(g):
+        return remote(gt.at[s, first_row], gback.at[me, first_row], hs_sem.at[s], hr_sem.at[me], ep=s)
+
+    def rows_out(g, c):
+        at = cols_of(c)
+        slot = back_slot(g)
+
+        def out(j):
+            s = g * per + lax.rem(col + 1 + j, per)
+
+            @pl.when(j == per - 1)
+            def _():
+                local(rg.at[rows(s), at], back.at[slot, rows(mine), at], br_sem.at[slot, c]).start()
+
+            @pl.when(j != per - 1)
+            def _():
+                back_copy(s, c, at).start()
+
+        loop(per, out)
+
+    def group(i, g):
         arrive(g)
         r = pl.ds(pl.multiple_of(g * rows_g, 16), rows_g)
         pg[...] = dot(xd[0, 0, r, :], wg[0], NN) + dot(xd[0, 1, r, :], wg[1], NN)
@@ -582,8 +662,8 @@
 
         def gates_in(j):
             s = g * per + j
-            local(gs.at[0], gr.at[s], gr_sem.at[s]).wait()
-            column = jnp.transpose(gr[s])
+            local(gs.at[0, first_row], gr.at[s, first_row], gr_sem.at[s]).wait()
+            column = jnp.transpose(jnp.broadcast_to(gr[s, 0:1, :], (8, 128)))
             gcol[rows(j), :] = jnp.broadcast_to(column[:cap, 0:1], (cap, 128))
 
         loop(per, gates_in)
@@ -602,50 +682,33 @@
 
         def part(c):
             at = cols_of(c)
-            for side, dst in ((other, give), (t, rg)):
-                dst[r, at] = (
+
+            @pl.when(i > 1)
+            def _():
+                exchange(i - 2, c).wait_send()
+
+            def half_rows_of(side):
+                return (
                     dot(gpgu[r, :units], wg[side, at, :], NT)
                     + dot(gpgu[r, units:], wu[side, at, :], NT)
                 ).astype(BF16)
-            exchange(g, c).start()
+
+            give[i % 2, :, at] = half_rows_of(other)
+            rg[r, at] = half_rows_of(t)
+            exchange(i, c).start()
 
         def gate_sum(j):
-            p = prod[rows(j), :]
-            gp[g * per + j, :, :cap] = dot(ones_units, p, NT, lax.Precision.HIGHEST)
+            gp[g * per + j, :, :cap] = lane_sums(prod[rows(j), :])
 
         def finish(c):
             at = cols_of(c)
-            exchange(g, c).wait_recv()
-            rg[r, at] = (rg[r, at].astype(F32) + got[r, at].astype(F32)).astype(BF16)
-
-            def out(j):
-                s = g * per + j
-                dest, slot = back_target(s)
-
-                @pl.when(dest == me)
-                def _():
-                    local(rg.at[rows(s), at], back.at[slot, rows(mine), at],
-                          br_sem.at[slot, c]).start()
-
-                @pl.when(dest != me)
-                def _():
-                    back_copy(s, c, at).start()
-
-            loop(per, out)
-
-        def column(c):
-            @pl.when(c < chunks)
-            def _():
-                part(c)
-
-            @pl.when(c > 0)
-            def _():
-                finish(c - 1)
-
-        loop(chunks + 1, column)
+            exchange(i, c).wait_recv()
+            rg[r, at] = (rg[r, at].astype(F32) + got[i % 2, :, at].astype(F32)).astype(BF16)
+
+            rows_out(g, c)
+
         loop(per, gate_sum)
         gate_exchange(g).start()
-        gate_exchange(g).wait_recv()
 
         def gates_out(j):
             s = g * per + j
@@ -653,23 +716,52 @@
 
             @pl.when(s == me)
             def _():
-                local(gt.at[s], gback.at[me], hr_sem.at[me]).start()
+                local(gt.at[s, first_row], gback.at[me, first_row], hr_sem.at[me]).start()
 
             @pl.when(s != me)
             def _():
                 gate_back(s).start()
 
-        loop(per, gates_out)
+        def column(c):
+            @pl.when(c < chunks)
+            def _():
+                part(c)
+
+            @pl.when(c == 1)
+            def _():
+                gate_exchange(g).wait_recv()
+                loop(per, gates_out)
+
+            @pl.when(c > 0)
+            def _():
+                finish(c - 1)
+
+        loop(chunks + 1, column)
 
     def comb_copy(q, at, c):
-        return remote(comb.at[q, :, at], far.at[:, at], cs_sem.at[q, c], cr_sem.at[c],
-                      ep=source_of(q))
+        there = far_inner * per + col
+        if q == 0:
+            return remote(comb.at[0, :, at], mid.at[:, at], cs_sem.at[0, c], mr_sem.at[c], ep=there)
+        return remote(comb.at[1, :, at], far.at[:, at], cs_sem.at[1, c], cr_sem.at[c], ep=there)
 
     def combine(q, c):
         at = cols_of(c)
-        local(near.at[0, :, at], back.at[q, :, at], br_sem.at[q, c]).wait()
+        gathered(q, c, at, br_sem)
+        gathered(q, c, at, bg_sem)
         comb[q, :, at] = dot(pq[q], back[q, :, at], TN).astype(BF16)
         comb_copy(q, at, c).start()
+
+    def merge_copy(at, c):
+        return remote(tx.at[1, :, at], far.at[:, at], ms_sem.at[c], cr_sem.at[c],
+                      ep=own_outer * per + col)
+
+    def merge(c):
+        at = cols_of(c)
+        gathered(3, c, at, br_sem)
+        close = dot(pm[...], back[3, own_block, at], TN)
+        local(far.at[:, at], mid.at[:, at], mr_sem.at[c]).wait()
+        tx[1, :, at] = (close + mid[:, at].astype(F32)).astype(BF16)
+        merge_copy(at, c).start()
 
     gp[...] = jnp.zeros_like(gp)
     for load in loads:
@@ -678,19 +770,60 @@
     def phase(i):
         @pl.when(inner & (i % 2 == 0))
         def _():
-            relay(i // 2)
-
-        @pl.when(inner & (i == planes - 1))
+            relay_start(i // 2)
+
+        @pl.when(inner & (i < planes - 1))
+        def _():
+            relay(i // 2, jnp.where(i == 1, chunks, 0), jnp.where(i == 2, 2 * chunks, chunks))
+
+        @pl.when(inner & (i == 1))
+        def _():
+            next_send(1)
+
+        @pl.when((outer & (i > 0)) | (i > 1))
+        def _():
+            scatter(
+                jnp.where(inner, 2, jnp.where(i == 1, 0, 1)),
+                jnp.where(i == 3, chunks, 0),
+                jnp.where(i == 1, 2 * chunks, chunks),
+            )
+
+        @pl.when(inner & (i == 2))
         def _():
             loop(chunks, lambda c: combine(0, c))
 
+        @pl.when(outer & (i == 3))
+        def _():
+            up(3)
+
         on_inner = jnp.where(i == 1, far_outer, jnp.where(i == 2, far_inner, own_outer))
-        on_outer = jnp.where(i == 1, own_inner, jnp.where(i == 2, far_outer, far_inner))
-        group(jnp.where(i == 0, z, jnp.where(inner, on_inner, on_outer)))
+        on_outer = jnp.where(i == 1, far_outer, jnp.where(i == 2, own_inner, far_inner))
+        group(i, jnp.where(i == 0, z, jnp.where(inner, on_inner, on_outer)))
+
+        @pl.when(outer & (i % 2 == 1))
+        def _():
+            up(i // 2)
+
+        @pl.when(outer & (i == 1))
+        def _():
+            next_send(1)
+
+        @pl.when(outer & (i < 2))
+        def _():
+            scatter(2, i * chunks, chunks)
 
     loop(planes, phase)
 
     acc[...] = jnp.zeros_like(acc)
+
+    @pl.when(inner)
+    def _():
+        remote(tg, rt.at[2], meta_s.at[1], meta_r.at[2], ep=my_relay).wait_recv()
+        plane_rows = lax.broadcasted_iota(jnp.int32, (rows_g, toks), 0) + z * rows_g
+        plane_rows = plane_rows.astype(F32)
+        pm[...] = jnp.where(
+            (plane_rows == rt[2, 0:1, :]) | (plane_rows == rt[2, 1:2, :]), 1.0, 0.0
+        ).astype(BF16)
 
     def grads(i):
         side = i // chunks
@@ -701,12 +834,16 @@
         wu[side, at, :] = q[:, units:]
         f = q.astype(F32)
         f = f * f
-        sqs[0, :, wide] = dot(ones_units, f[:, :units], NT, lax.Precision.HIGHEST)
-        sqs[1, :, wide] = dot(ones_units, f[:, units:], NT, lax.Precision.HIGHEST)
+        sqs[0, :, wide] = lane_sums(f[:, :units])
+        sqs[1, :, wide] = lane_sums(f[:, units:])
         d = dot(wt[...], xd[1, side, :, at], TN).astype(BF16)
         wd[:, wide] = d
         d = d.astype(F32)
-        acc[...] += d * d
+        acc[...] += lane_sums(d * d)
+
+        @pl.when(inner & (i % 2 == 0))
+        def _():
+            merge(i // 2)
 
         @pl.when(inner & (i % 2 == 1))
         def _():
@@ -722,17 +859,16 @@
         store.start()
     squares = remote(sqs, sqr, e_sem.at[0], e_sem.at[1], tp=other)
     squares.start()
-    sum_down = dot(jnp.ones((8, tile), F32), acc[...], NT, lax.Precision.HIGHEST)
-    sqd[...] = sum_down[0:1, :] / (2 * share)
+    sqd[...] = acc[0:1, :] / (2 * share)
     squares.wait()
     sqg[...] = (sqs[0, 0:1, :] + sqr[0, 0:1, :]) / full_units
     squ[...] = (sqs[1, 0:1, :] + sqr[1, 0:1, :]) / full_units
 
-    loop(n, lambda e: local(gt.at[e], gback.at[e], hr_sem.at[e]).wait())
+    loop(n, lambda e: local(gt.at[e, first_row], gback.at[e, first_row], hr_sem.at[e]).wait())
     slots = lax.broadcasted_iota(jnp.int32, (cap, toks), 0)
 
     def look_up(e, carry):
-        column = jnp.transpose(gback[e])[:cap, 0:1]
+        column = jnp.transpose(jnp.broadcast_to(gback[e, 0:1, :], (8, 128)))[:cap, 0:1]
         at = (slots + e * cap).astype(F32)
         return tuple(
             v + jnp.where(at == tg[k:k + 1, :], column, 0.0) for k, v in enumerate(carry)
@@ -743,37 +879,40 @@
     for k in range(2):
         ggate[k:k + 1, :] = jnp.sum(found[k], axis=0, keepdims=True)
 
-    def last(c):
-        at = cols_of(c)
-        local(near.at[0, :, at], back.at[2, :, at], br_sem.at[2, c]).wait()
-        close = dot(pn[...], back[2, :, at], TN)
-        local(far.at[:, at], far.at[:, at], cr_sem.at[c]).wait()
-        gout[:, at] = (close + far[:, at].astype(F32)).astype(BF16)
-        local(gout.at[:, at], gtok.at[:, at], go_sem.at[c]).start()
-
-    loop(chunks, last)
-
-    for store in stores:
-        store.wait()
-    loop(chunks, lambda c: local(gout.at[:, cols_of(c)], gtok.at[:, cols_of(c)], go_sem.at[c]).wait())
-
     meta.wait_send()
     for which in range(2):
         loop(chunks, lambda c, which=which: raw_copy(which, c).wait_send())
 
-    def drain_near(d):
-        @pl.when(d != mine)
+    @pl.when(outer)
+    def _():
+        close_meta.wait_send()
+        for slot in (0, 1, 3):
+            up_copy(slot, 0, pl.ds(0, share)).wait_send()
+
+    for which in range(2):
+        next_copy(which, 0, pl.ds(0, share)).wait_send()
+
+    def drain_near(j):
+        @pl.when(j != col)
         def _():
             for which in range(2):
-                near_copy(which, d).wait_send()
-
-            @pl.when(inner)
-            def _():
-                for q in range(2):
-                    for which in range(2):
-                        fwd_copy(q, which, d, pl.ds(0, share)).wait_send()
-
-    loop(half, drain_near)
+                near_copy(which, j).wait_send()
+
+    loop(per, drain_near)
+
+    def drain_spread(j):
+        for q in range(3):
+            for which in range(2):
+                @pl.when(j != col)
+                def _(q=q, which=which):
+                    spread_copy(raw.at[q, which, rows(j)], q, which, j, pl.ds(0, share)).wait_send()
+
+                if q < 2:
+                    @pl.when(inner & (j == col))
+                    def _(q=q, which=which):
+                        cross_copy(q, which, 0, pl.ds(0, share)).wait_send()
+
+    loop(per, drain_spread)
 
     def drain(k):
         d = peer(k)
@@ -785,24 +924,53 @@
     def drain_rows(s):
         for which in range(2):
             pair_copy(which, s).wait_send()
-        dest, _ = back_target(s)
-
-        @pl.when(dest != me)
+
+        @pl.when(s % per != col)
         def _():
             back_copy(s, 0, pl.ds(0, share)).wait_send()
 
     loop(n, drain_rows)
 
     def drain_group(g):
-        loop(chunks, lambda c: exchange(g, c).wait_send())
         gate_exchange(g).wait_send()
 
+        @pl.when(g >= planes - 2)
+        def _():
+            loop(chunks, lambda c: exchange(g, c).wait_send())
+
     loop(planes, drain_group)
+
+    def last(c):
+        at = cols_of(c)
+
+        def finish_rows(part):
+            gathered(2, c, at, br_sem)
+            close = dot(pn[part, :], back[2, part, at], TN)
+            local(far.at[:, at], far.at[:, at], cr_sem.at[c]).wait()
+            tx[0, :, at] = (close + far[:, at].astype(F32)).astype(BF16)
+
+        @pl.when(inner)
+        def _():
+            gathered(2, c, at, bg_sem)
+            finish_rows(pl.ds(0, hr))
+
+        @pl.when(outer)
+        def _():
+            finish_rows(own_block)
+
+        local(tx.at[0, :, at], gtok.at[:, at], go_sem.at[c]).start()
+
+    loop(chunks, last)
 
     @pl.when(inner)
     def _():
         for q in range(2):
             loop(chunks, lambda c, q=q: comb_copy(q, cols_of(c), c).wait_send())
+        loop(chunks, lambda c: merge_copy(cols_of(c), c).wait_send())
+
+    for store in stores:
+        store.wait()
+    loop(chunks, lambda c: local(tx.at[0, :, cols_of(c)], gtok.at[:, cols_of(c)], go_sem.at[c]).wait())
 
 
 def relay_scratch(n, planes, cap, units, share, tile, toks):
@@ -811,24 +979,26 @@
     hr = n // 2 * cap
     chunks = share // tile
     half = n // 2
+    per = n // planes
     width = 2 * share
     arrays = [
         ((2, 2, total, share), BF16), ((2, toks, share), BF16), ((hr, toks), BF16),
-        ((2, hr, share), BF16), ((8, toks), F32), ((2, 8, toks), F32), ((2, hr, toks), BF16),
-        ((2, 2, toks, share), BF16), ((2, 2, hr, share), BF16),
+        ((2, hr, share), BF16), ((8, toks), F32), ((3, 8, toks), F32), ((2, hr, toks), BF16),
+        ((3, 2, toks, share), BF16), ((2, 2, hr, share), BF16),
         ((2, share, units), BF16), ((2, share, units), BF16), ((units, width), BF16),
         ((n, 8, 128), F32), ((n, 8, 128), F32), ((group, 128), F32),
         ((group, units), F32), ((group, units), F32), ((group, units), F32),
         ((total, 2 * units), BF16), ((total, units), BF16),
-        ((total, share), BF16), ((total, share), BF16), ((total, share), BF16),
+        ((2, group, share), BF16), ((2, group, share), BF16), ((total, share), BF16),
         ((n, 8, 128), F32), ((n, 8, 128), F32), ((n, 8, 128), F32), ((n, 8, 128), F32),
-        ((3, hr, share), BF16), ((2, toks, share), BF16), ((toks, share), BF16),
-        ((toks, share), BF16), ((2, 8, width), F32), ((2, 8, width), F32), ((units, tile), F32),
+        ((4, hr, share), BF16), ((2, toks, share), BF16), ((toks, share), BF16),
+        ((toks, share), BF16), ((group, toks), BF16), ((2, 8, width), F32), ((2, 8, width), F32), ((8, units), F32),
     ]
     sems = [
-        (3,), (2,), (2, chunks), (2, 2, chunks), (1,), (2,), (2, half), (2, n), (2, 2, half),
+        (3,), (2,), (2, chunks), (3, 2, chunks), (2,), (3,), (2, per), (2, n), (3, 2, per),
         (n,), (n,), (2, n), (2, n), (planes, chunks), (planes, chunks), (planes,), (planes,),
-        (n,), (3, chunks), (2, chunks), (chunks,), (n,), (n,), (3,), (2,), (chunks,),
+        (n,), (4, chunks), (2, chunks), (chunks,), (n,), (n,), (3,), (2,), (chunks,),
+        (2,), (chunks,), (chunks,), (4,), (3, chunks),
     ]
     size = 0
     for dims, kind in arrays:
@@ -882,7 +1052,7 @@
     tile = 512
     units = gate_w.shape[2]
     _, _, size = relay_scratch(n_ep, PLANES, cap, units, share, tile, tok_rows)
-    if n_ep % PLANES == 0 and tok_rows < n_ep // 2 * cap and size + (3 << 20) < VMEM_BYTES:
+    if n_ep % PLANES == 0 and tok_rows < n_ep // 2 * cap and size + (1 << 20) < VMEM_BYTES:
         gtok, ggate, ggw, guw, gdw, sqg, squ, sqd = fused_relay(
             n_ep, PLANES, cap, tok_rows, tile, tokens, cotangent, gates, experts,
             gate_w[0], up_w[0], down_w[0],

time: 216 us -> 191 us (0.88)
  Pallas kernels: 199 us -> 175 us
    pallas_call x1, Pallas kernels: 199 us -> 175 us  [fused_relay(): pl.pallas_call(functools.partial(relay_kernel, n, planes, cap, units, sha...]
where the time goes in v2:
time: 191 us; the launch traced here: 190 us
  Pallas kernels  175 us (92%)
  local copies, waits for them, and re-layouts  14.1 us (7%)
    pallas_call x1, Pallas kernels, fused_relay(): pl.pallas_call(functools.partial(relay_kernel, n, planes, cap, units, sha...  175 us
    unnamed x18, local copies, waits for them, and re-layouts  14.1 us

profile of v2, /device:TPU:15, one launch (start us, length us, event | category | flops | bytes accessed | tf_op | source)
XLA Modules:
  0.0 189.9 jit_solution(5571587947229393030)
XLA Ops:
  0.6 175.2 %shard_map.134 = (bf16[256,2048]{1,0:T(8,128)(2,1)}, f32[2,256]{1,0:T(2,128)}, bf16[2,2048,384]{2,1,0:T(8,128)(2,1)}, bf16[2,2048,384]{2,1,0:T(8,128)(2,1)}, bf1...) custom-call(bf16[256,4096]{1,0:T(8,128)(2,1)} %tok.1, ...), custom_call_target="tpu_custom_call" | custom-call | tf_op jit(solution)/shard_map/pallas_call | solution.py:1020
  175.9 2.3 %copy.23 = bf16[256,2048]{1,0:T(8,128)(2,1)} copy(bf16[256,2048]{1,0:T(8,128)(2,1)} %get-tuple-element.32) | data formatting | bytes 2097152
  178.2 1.3 copy.24
  179.4 0.0 copy-start.1
  179.4 4.0 %copy.25 = bf16[1,4096,384]{2,1,0:T(8,128)(2,1)} copy(bf16[1,4096,384]{2,1,0:T(8,128)(2,1)} %bitcast.11) | data formatting | bytes 6291456
  183.4 0.0 copy-done.1
  183.5 0.0 copy-start
  183.5 1.7 copy.26
  185.1 1.4 copy-done
  186.5 0.0 copy-start.3
  186.5 0.0 copy-start.2
  186.5 0.0 copy-start.4
  186.5 1.7 copy.27
  188.1 0.0 copy-done.3
  188.2 0.6 copy.28
  188.8 0.0 copy-done.2
  188.8 0.6 copy.29
  189.4 0.0 copy-done.4
  189.4 0.6 copy.30
Async XLA Ops:
  179.4 4.0 %copy-start.1 = (bf16[2,2048,384]{2,1,0:T(8,128)(2,1)S(1)}, bf16[2,2048,384]{2,1,0:T(8,128)(2,1)}, u32[]{:S(2)}) copy-start(bf16[2,2048,384]{2,1,0:T(8,128)(2,1)} %get-tuple-element.19) | copy-start | bytes 9437188
  183.5 3.0 %copy-start = (bf16[384,4096]{1,0:T(8,128)(2,1)S(1)}, bf16[384,4096]{1,0:T(8,128)(2,1)}, u32[]{:S(2)}) copy-start(bf16[384,4096]{1,0:T(8,128)(2,1)} %get-tuple-element.20) | copy-start | bytes 9437188
  186.5 1.7 copy-start.3
  186.5 2.3 %copy-start.2 = (f32[1,4096]{1,0:T(1,128)S(1)}, f32[1,4096]{1,0:T(1,128)}, u32[]{:S(2)}) copy-start(f32[1,4096]{1,0:T(1,128)} %get-tuple-element.38) | copy-start | bytes 49156
  186.5 2.9 %copy-start.4 = (f32[1,384]{1,0:T(1,128)S(1)}, f32[1,384]{1,0:T(1,128)}, u32[]{:S(2)}) copy-start(f32[1,384]{1,0:T(1,128)} %get-tuple-element.39) | copy-start | bytes 4612

commit v3 on v2

--- a/solution.py
+++ b/solution.py
@@ -332,12 +332,12 @@
 def relay_kernel(
     n, planes, cap, units, share, tile, toks, full_units,
     tok, cot, gates, experts, wg_in, wu_in, wd_in,
-    gtok, ggate, ggw, guw, gdw, sqg, squ, sqd,
+    gtok, ggate_out, ggw, guw, gdw, sqg_out, squ_out, sqd_out,
     xd, tx, pn, near, tg, rt, pq, raw, fwd, wg, wu, wd, gs, gr, gcol, pg, pu, prod, gpgu, wt,
-    give, got, rg, gp, gpp, gt, gback, back, comb, far, mid, pm, sqs, sqr, acc,
+    give, got, rg, gp, gpp, gt, gback, back, comb, far, mid, pm, sqs, sqr, acc, ggate, sqg, squ, sqd,
     w_sem, t_sem, raw_s, raw_r, meta_s, meta_r, s_sem, r_sem, f_sem, gs_sem, gr_sem, ps_sem, pr_sem,
     xs_sem, xr_sem, qs_sem, qr_sem, bs_sem, br_sem, cs_sem, cr_sem, hs_sem, hr_sem, o_sem, e_sem, go_sem,
-    n_sem, ms_sem, mr_sem, bf_sem, bg_sem,
+    n_sem, ms_sem, mr_sem, bf_sem, small_sem,
 ):
     me = lax.axis_index("ep")
     t = lax.axis_index("tp")
@@ -505,6 +505,7 @@
     near_send(0)
     next_send(0)
     near_send(1)
+    next_send(1)
 
     for load in loads:
         load.start()
@@ -615,21 +616,28 @@
 
     def back_copy(s, c, at):
         slot = back_slot(s // per)
+        plane = jnp.where(straight(s // per), own_inner, z)
         return remote(rg.at[rows(s), at], back.at[slot, rows(mine), at], bs_sem.at[s],
-                      br_sem.at[slot, c], ep=z * per + s % per)
-
-    def gathered(slot, c, at, sem):
-        local(near.at[0, block, at], back.at[slot, block, at], sem.at[slot, c]).wait()
+                      br_sem.at[back_mark(s // per), c], ep=plane * per + s % per)
+
+    def straight(g):
+        return outer & (g == far_inner)
+
+    def back_mark(g):
+        return jnp.where(straight(g), 5, back_slot(g))
+
+    def gathered(mark, c, at):
+        local(near.at[0, block, at], back.at[0, block, at], br_sem.at[mark, c]).wait()
 
     def up_copy(slot, c, at):
         to = jnp.where(slot == 3, 2, slot)
         return remote(back.at[slot, own_block, at], back.at[to, own_block, at],
-                      bf_sem.at[slot], bg_sem.at[to, c], ep=own_inner * per + col)
+                      bf_sem.at[slot], br_sem.at[4 + to, c], ep=own_inner * per + col)
 
     def up(slot):
         def step(c):
             at = cols_of(c)
-            gathered(slot, c, at, br_sem)
+            gathered(slot, c, at)
             up_copy(slot, c, at).start()
 
         loop(chunks, step)
@@ -644,11 +652,11 @@
         def out(j):
             s = g * per + lax.rem(col + 1 + j, per)
 
-            @pl.when(j == per - 1)
+            @pl.when((j == per - 1) & jnp.logical_not(straight(g)))
             def _():
                 local(rg.at[rows(s), at], back.at[slot, rows(mine), at], br_sem.at[slot, c]).start()
 
-            @pl.when(j != per - 1)
+            @pl.when((j != per - 1) | straight(g))
             def _():
                 back_copy(s, c, at).start()
 
@@ -746,8 +754,8 @@
 
     def combine(q, c):
         at = cols_of(c)
-        gathered(q, c, at, br_sem)
-        gathered(q, c, at, bg_sem)
+        gathered(q, c, at)
+        gathered(4 + q, c, at)
         comb[q, :, at] = dot(pq[q], back[q, :, at], TN).astype(BF16)
         comb_copy(q, at, c).start()
 
@@ -757,7 +765,7 @@
 
     def merge(c):
         at = cols_of(c)
-        gathered(3, c, at, br_sem)
+        gathered(3, c, at)
         close = dot(pm[...], back[3, own_block, at], TN)
         local(far.at[:, at], mid.at[:, at], mr_sem.at[c]).wait()
         tx[1, :, at] = (close + mid[:, at].astype(F32)).astype(BF16)
@@ -771,46 +779,40 @@
         @pl.when(inner & (i % 2 == 0))
         def _():
             relay_start(i // 2)
-
-        @pl.when(inner & (i < planes - 1))
-        def _():
-            relay(i // 2, jnp.where(i == 1, chunks, 0), jnp.where(i == 2, 2 * chunks, chunks))
-
-        @pl.when(inner & (i == 1))
-        def _():
-            next_send(1)
-
-        @pl.when((outer & (i > 0)) | (i > 1))
-        def _():
-            scatter(
-                jnp.where(inner, 2, jnp.where(i == 1, 0, 1)),
-                jnp.where(i == 3, chunks, 0),
-                jnp.where(i == 1, 2 * chunks, chunks),
-            )
+            relay(i // 2, 0, chunks)
+
+        @pl.when((inner & (i == 2)) | (outer & (i == 0)))
+        def _():
+            scatter(2, 0, chunks)
+
+        @pl.when(inner & ((i == 1) | (i == 2)))
+        def _():
+            relay(i - 1, chunks, chunks)
+
+        @pl.when((inner & (i == 2)) | (outer & (i == 1)))
+        def _():
+            scatter(2, chunks, chunks)
+
+        @pl.when(outer & (i > 0))
+        def _():
+            scatter(jnp.where(i == 3, 1, 0), jnp.where(i == 1, 0, chunks), chunks)
+
+        on_inner = jnp.where(i == 1, far_outer, jnp.where(i == 2, far_inner, own_outer))
+        on_outer = jnp.where(i == 1, own_inner, jnp.where(i == 2, far_outer, far_inner))
+        group(i, jnp.where(i == 0, z, jnp.where(inner, on_inner, on_outer)))
 
         @pl.when(inner & (i == 2))
         def _():
             loop(chunks, lambda c: combine(0, c))
 
-        @pl.when(outer & (i == 3))
-        def _():
+        @pl.when(outer & (i == 2))
+        def _():
+            scatter(1, 0, chunks)
+
+        @pl.when(outer & (i == 2))
+        def _():
+            up(0)
             up(3)
-
-        on_inner = jnp.where(i == 1, far_outer, jnp.where(i == 2, far_inner, own_outer))
-        on_outer = jnp.where(i == 1, far_outer, jnp.where(i == 2, own_inner, far_inner))
-        group(i, jnp.where(i == 0, z, jnp.where(inner, on_inner, on_outer)))
-
-        @pl.when(outer & (i % 2 == 1))
-        def _():
-            up(i // 2)
-
-        @pl.when(outer & (i == 1))
-        def _():
-            next_send(1)
-
-        @pl.when(outer & (i < 2))
-        def _():
-            scatter(2, i * chunks, chunks)
 
     loop(planes, phase)
 
@@ -863,6 +865,14 @@
     squares.wait()
     sqg[...] = (sqs[0, 0:1, :] + sqr[0, 0:1, :]) / full_units
     squ[...] = (sqs[1, 0:1, :] + sqr[1, 0:1, :]) / full_units
+    small = [
+        local(a, b, small_sem.at[i])
+        for i, (a, b) in enumerate(
+            ((sqg, sqg_out), (squ, squ_out), (sqd, sqd_out), (ggate, ggate_out))
+        )
+    ]
+    for copy in small[:3]:
+        copy.start()
 
     loop(n, lambda e: local(gt.at[e, first_row], gback.at[e, first_row], hr_sem.at[e]).wait())
     slots = lax.broadcasted_iota(jnp.int32, (cap, toks), 0)
@@ -878,6 +888,7 @@
     found = lax.fori_loop(0, n, look_up, (zero, zero))
     for k in range(2):
         ggate[k:k + 1, :] = jnp.sum(found[k], axis=0, keepdims=True)
+    small[3].start()
 
     meta.wait_send()
     for which in range(2):
@@ -886,7 +897,7 @@
     @pl.when(outer)
     def _():
         close_meta.wait_send()
-        for slot in (0, 1, 3):
+        for slot in (0, 3):
             up_copy(slot, 0, pl.ds(0, share)).wait_send()
 
     for which in range(2):
@@ -925,7 +936,7 @@
         for which in range(2):
             pair_copy(which, s).wait_send()
 
-        @pl.when(s % per != col)
+        @pl.when((s % per != col) | straight(s // per))
         def _():
             back_copy(s, 0, pl.ds(0, share)).wait_send()
 
@@ -944,14 +955,14 @@
         at = cols_of(c)
 
         def finish_rows(part):
-            gathered(2, c, at, br_sem)
+            gathered(2, c, at)
             close = dot(pn[part, :], back[2, part, at], TN)
             local(far.at[:, at], far.at[:, at], cr_sem.at[c]).wait()
             tx[0, :, at] = (close + far[:, at].astype(F32)).astype(BF16)
 
         @pl.when(inner)
         def _():
-            gathered(2, c, at, bg_sem)
+            gathered(6, c, at)
             finish_rows(pl.ds(0, hr))
 
         @pl.when(outer)
@@ -968,6 +979,8 @@
             loop(chunks, lambda c, q=q: comb_copy(q, cols_of(c), c).wait_send())
         loop(chunks, lambda c: merge_copy(cols_of(c), c).wait_send())
 
+    for copy in small:
+        copy.wait()
     for store in stores:
         store.wait()
     loop(chunks, lambda c: local(tx.at[0, :, cols_of(c)], gtok.at[:, cols_of(c)], go_sem.at[c]).wait())
@@ -993,12 +1006,13 @@
         ((n, 8, 128), F32), ((n, 8, 128), F32), ((n, 8, 128), F32), ((n, 8, 128), F32),
         ((4, hr, share), BF16), ((2, toks, share), BF16), ((toks, share), BF16),
         ((toks, share), BF16), ((group, toks), BF16), ((2, 8, width), F32), ((2, 8, width), F32), ((8, units), F32),
+        ((2, toks), F32), ((1, width), F32), ((1, width), F32), ((1, units), F32),
     ]
     sems = [
         (3,), (2,), (2, chunks), (3, 2, chunks), (2,), (3,), (2, per), (2, n), (3, 2, per),
         (n,), (n,), (2, n), (2, n), (planes, chunks), (planes, chunks), (planes,), (planes,),
-        (n,), (4, chunks), (2, chunks), (chunks,), (n,), (n,), (3,), (2,), (chunks,),
-        (2,), (chunks,), (chunks,), (4,), (3, chunks),
+        (n,), (7, chunks), (2, chunks), (chunks,), (n,), (n,), (3,), (2,), (chunks,),
+        (2,), (chunks,), (chunks,), (4,), (4,),
     ]
     size = 0
     for dims, kind in arrays:
@@ -1030,7 +1044,7 @@
             shape((1, units), F32),
         ),
         in_specs=[any_spec, any_spec, vmem, vmem, any_spec, any_spec, any_spec],
-        out_specs=(any_spec, vmem, any_spec, any_spec, any_spec, vmem, vmem, vmem),
+        out_specs=(any_spec,) * 8,
         scratch_shapes=[pltpu.VMEM(dims, kind) for dims, kind in arrays]
         + [pltpu.SemaphoreType.DMA(dims) for dims in sems],
         compiler_params=pltpu.CompilerParams(

time: 191 us -> 184 us (0.963); the launches traced: 190 us -> 181 us
  Pallas kernels: 175 us -> 166 us
    pallas_call x1, Pallas kernels: 175 us -> 166 us  [fused_relay(): pl.pallas_call(functools.partial(relay_kernel, n, planes, cap, units, sha...]
where the time goes in v3:
time: 184 us; the launch traced here: 181 us
  Pallas kernels  166 us (90%)
  local copies, waits for them, and re-layouts  14.1 us (8%)
    pallas_call x1, Pallas kernels, fused_relay(): pl.pallas_call(functools.partial(relay_kernel, n, planes, cap, units, sha...  166 us
    unnamed x18, local copies, waits for them, and re-layouts  14.1 us

profile of v3, /device:TPU:15, one launch (start us, length us, event | category | flops | bytes accessed | tf_op | source)
XLA Modules:
  0.0 180.5 jit_solution(9291707266706511562)
XLA Ops:
  0.6 165.8 %shard_map.134 = (bf16[256,2048]{1,0:T(8,128)(2,1)}, f32[2,256]{1,0:T(2,128)}, bf16[2,2048,384]{2,1,0:T(8,128)(2,1)}, bf16[2,2048,384]{2,1,0:T(8,128)(2,1)}, bf1...) custom-call(bf16[256,4096]{1,0:T(8,128)(2,1)} %tok.1, ...), custom_call_target="tpu_custom_call" | custom-call | tf_op jit(solution)/shard_map/pallas_call | solution.py:1034
  166.4 2.3 %copy.23 = bf16[256,2048]{1,0:T(8,128)(2,1)} copy(bf16[256,2048]{1,0:T(8,128)(2,1)} %get-tuple-element.32) | data formatting | bytes 2097152
  168.7 1.3 copy.24
  170.0 0.0 copy-start.1
  170.0 4.0 %copy.25 = bf16[1,4096,384]{2,1,0:T(8,128)(2,1)} copy(bf16[1,4096,384]{2,1,0:T(8,128)(2,1)} %bitcast.11) | data formatting | bytes 6291456
  174.0 0.0 copy-done.1
  174.0 0.0 copy-start
  174.0 1.7 copy.26
  175.7 1.4 copy-done
  177.0 0.0 copy-start.3
  177.1 0.0 copy-start.2
  177.1 0.0 copy-start.4
  177.1 1.7 copy.27
  178.7 0.0 copy-done.3
  178.7 0.6 copy.28
  179.3 0.0 copy-done.2
  179.3 0.6 copy.29
  179.9 0.0 copy-done.4
  179.9 0.6 copy.30
Async XLA Ops:
  170.0 4.0 %copy-start.1 = (bf16[2,2048,384]{2,1,0:T(8,128)(2,1)S(1)}, bf16[2,2048,384]{2,1,0:T(8,128)(2,1)}, u32[]{:S(2)}) copy-start(bf16[2,2048,384]{2,1,0:T(8,128)(2,1)} %get-tuple-element.19) | copy-start | bytes 9437188
  174.0 3.0 %copy-start = (bf16[384,4096]{1,0:T(8,128)(2,1)S(1)}, bf16[384,4096]{1,0:T(8,128)(2,1)}, u32[]{:S(2)}) copy-start(bf16[384,4096]{1,0:T(8,128)(2,1)} %get-tuple-element.20) | copy-start | bytes 9437188
  177.0 1.7 copy-start.3
  177.1 2.3 %copy-start.2 = (f32[1,4096]{1,0:T(1,128)S(1)}, f32[1,4096]{1,0:T(1,128)}, u32[]{:S(2)}) copy-start(f32[1,4096]{1,0:T(1,128)} %get-tuple-element.38) | copy-start | bytes 49156
  177.1 2.9 %copy-start.4 = (f32[1,384]{1,0:T(1,128)S(1)}, f32[1,384]{1,0:T(1,128)}, u32[]{:S(2)}) copy-start(f32[1,384]{1,0:T(1,128)} %get-tuple-element.39) | copy-start | bytes 4612
